TPU v7x, 32 devices: a whole 2x2x4 slice. The times are simulated.
32 devices in a mesh: sp: 8 (over z, y), tp: 4 (over x, core).
Axes of the slice: x: 2, y: 2, z: 4, core: 2. Of those that a mesh axis runs over, the one named last changes fastest.
Arguments:
- resid: bfloat16 [2048, 2048], P(('sp', 'tp')), may hold values from -6 to 6
- query_a: bfloat16 [2048, 4, 128], P('sp', 'tp')
- key_a: bfloat16 [2048, 4, 128], P('sp', 'tp')
- value_a: bfloat16 [2048, 4, 128], P('sp', 'tp'), may hold values from -6 to 6
- query_b: bfloat16 [2048, 4, 256], P('sp', 'tp')
- key_b: bfloat16 [2048, 4, 256], P('sp', 'tp')
- value_b: bfloat16 [2048, 4, 128], P('sp', 'tp'), may hold values from -6 to 6
- lambda_a: float32 [4], P('tp'), may hold values from 0.3 to 0.8
- lambda_b: float32 [4], P('tp'), may hold values from 0.3 to 0.8
- head_gain: float32 [128], replicated, may hold values from 0.1 to 1.9
- out_weight: bfloat16 [1024, 2048], replicated, may hold values from -0.1875 to 0.1875
- norm_gain: float32 [2048], replicated, may hold values from 0.1 to 1.9
- expert_ids: int32 [2048, 4], P(('sp', 'tp')), may hold values from 0 to 31, all different within a row; in each aligned block of 64 rows (0 to 63, 64 to 127, ...) at most 16 rows name the same one
- expert_mix: float32 [2048, 4], P(('sp', 'tp')), may hold values from 0.2 to 1
- gate_experts: bfloat16 [32, 2048, 1024], P(('sp', 'tp')), may hold values from -0.125 to 0.125
- up_experts: bfloat16 [32, 2048, 1024], P(('sp', 'tp')), may hold values from -0.125 to 0.125
- down_experts: bfloat16 [32, 1024, 2048], P(('sp', 'tp')), may hold values from -0.1875 to 0.1875
- shared_gate: bfloat16 [2048, 512], replicated, may hold values from -0.125 to 0.125
- shared_up: bfloat16 [2048, 512], replicated, may hold values from -0.125 to 0.125
- shared_down: bfloat16 [512, 2048], replicated, may hold values from -0.25 to 0.25
Outputs:
- layer_out: bfloat16 [2048, 2048], P(('sp', 'tp'))
Inputs may be any that keep to these rules, and one draw needn't show every extreme that they name: `expert_ids`: in each aligned block of 64 rows (the rows of one device) no expert is named more than 16 times, a bound that some block reaches.
All inputs are finite; a program needn't handle non-finite values.
Results may differ from a plain program's by a relative error of at most 0.017.
Values may be sent and summed in bfloat16 or wider, within the bound.
No kernel may reach another device: no remote copies, remote signals or barrier semaphores. Data moves between devices by JAX's collectives and lax.ppermute only.
A program may use at most 128 MiB of HBM per device.

v0:
```python
import math
import jax
import jax.numpy as jnp
from jax import lax
from jax.sharding import PartitionSpec as P

NEG_FILL = -1e30
EPSILON = 1e-05
HEAD_SCALE = 0.8
KEY_SPAN = 2048


def swiglu_rows(row_set, w_gate, w_up, w_down):
    gate_val = jnp.dot(row_set, w_gate, preferred_element_type=jnp.float32)
    up_val = jnp.dot(row_set, w_up, preferred_element_type=jnp.float32)
    hidden = (jax.nn.silu(gate_val) * up_val).astype(jnp.bfloat16)
    return jnp.dot(hidden, w_down, preferred_element_type=jnp.float32)


def online_update(state, query_map, key_map, value_block, causal, scaling):
    row_top, denoms, numerator = state
    scores = (
        jnp.einsum("qhd,khd->hqk", query_map, key_map, preferred_element_type=jnp.float32) * scaling
    )
    scores = jnp.where(causal, scores, NEG_FILL)
    new_top = jnp.maximum(row_top, jnp.max(scores, axis=2))
    exponent = jnp.where(causal, jnp.exp(scores - new_top[:, :, None]), 0.0)
    shrink = jnp.exp(row_top - new_top)
    denoms = denoms * shrink + jnp.sum(exponent, axis=2)
    numerator = numerator * jnp.transpose(shrink)[:, :, None] + jnp.einsum(
        "hqk,khe->qhe",
        exponent.astype(jnp.bfloat16),
        value_block,
        preferred_element_type=jnp.float32,
    )
    return (new_top, denoms, numerator)


def group_update(states, queries, key_block, value_block, causal):
    map_width = queries.shape[2] // 2
    scaling = map_width ** (-0.5)
    first_state = online_update(
        states[0],
        queries[:, :, :map_width],
        key_block[:, :, :map_width],
        value_block,
        causal,
        scaling,
    )
    second_state = online_update(
        states[1],
        queries[:, :, map_width:],
        key_block[:, :, map_width:],
        value_block,
        causal,
        scaling,
    )
    return (first_state, second_state)


def empty_state(query_rows, head_count, value_width):
    single = (
        jnp.full((head_count, query_rows), NEG_FILL, jnp.float32),
        jnp.zeros((head_count, query_rows), jnp.float32),
        jnp.zeros((query_rows, head_count, value_width), jnp.float32),
    )
    return (single, single)


def finish_group(states, lambdas, head_gain):
    first_out = states[0][2] / jnp.transpose(states[0][1])[:, :, None]
    second_out = states[1][2] / jnp.transpose(states[1][1])[:, :, None]
    differ = first_out - lambdas[None, :, None] * second_out
    scale_rms = lax.rsqrt(jnp.mean(differ * differ, axis=2, keepdims=True) + EPSILON)
    return (differ * scale_rms * head_gain[None, None, :] * HEAD_SCALE).astype(jnp.bfloat16)


def per_device(
    resid,
    query_a,
    key_a,
    value_a,
    query_b,
    key_b,
    value_b,
    lambda_a,
    lambda_b,
    head_gain,
    out_weight,
    norm_gain,
    expert_ids,
    expert_mix,
    gate_experts,
    up_experts,
    down_experts,
    shared_gate,
    shared_up,
    shared_down,
):
    query_rows = query_a.shape[0]
    value_width = value_a.shape[2]
    query_pos = lax.axis_index("sp") * query_rows + jnp.arange(query_rows, dtype=jnp.int32)
    start_state = (
        empty_state(query_rows, query_a.shape[1], value_width),
        empty_state(query_rows, query_b.shape[1], value_width),
    )
    key_piece_a = lax.all_gather(key_a, "sp", axis=0, tiled=True)
    value_piece_a = lax.all_gather(value_a, "sp", axis=0, tiled=True)
    key_piece_b = lax.all_gather(key_b, "sp", axis=0, tiled=True)
    value_piece_b = lax.all_gather(value_b, "sp", axis=0, tiled=True)
    piece_rows = key_piece_a.shape[0]
    step_rows = math.gcd(piece_rows, KEY_SPAN)

    def one_step(step_index, inner_state):
        begin_row = step_index * step_rows
        key_pos = begin_row + jnp.arange(step_rows, dtype=jnp.int32)
        causal = (key_pos[None, :] <= query_pos[:, None])[None]
        part_a = group_update(
            inner_state[0],
            query_a,
            lax.dynamic_slice_in_dim(key_piece_a, begin_row, step_rows, 0),
            lax.dynamic_slice_in_dim(value_piece_a, begin_row, step_rows, 0),
            causal,
        )
        part_b = group_update(
            inner_state[1],
            query_b,
            lax.dynamic_slice_in_dim(key_piece_b, begin_row, step_rows, 0),
            lax.dynamic_slice_in_dim(value_piece_b, begin_row, step_rows, 0),
            causal,
        )
        return (part_a, part_b)

    state_a, state_b = lax.fori_loop(0, piece_rows // step_rows, one_step, start_state)
    heads_a = finish_group(state_a, lambda_a, head_gain)
    heads_b = finish_group(state_b, lambda_b, head_gain)
    tok_dev = resid.shape[0]
    back_a, back_b = (
        lax.all_to_all(heads_a, "tp", split_axis=0, concat_axis=1, tiled=True),
        lax.all_to_all(heads_b, "tp", split_axis=0, concat_axis=1, tiled=True),
    )
    joined = jnp.concatenate([back_a.reshape(tok_dev, -1), back_b.reshape(tok_dev, -1)], axis=1)
    project = jnp.dot(joined, out_weight, preferred_element_type=jnp.float32)
    middle = (resid.astype(jnp.float32) + project).astype(jnp.bfloat16)
    middle_f = middle.astype(jnp.float32)
    normed = (
        middle_f
        * lax.rsqrt(jnp.mean(middle_f * middle_f, axis=1, keepdims=True) + EPSILON)
        * norm_gain[None, :]
    ).astype(jnp.bfloat16)
    shared = swiglu_rows(normed, shared_gate, shared_up, shared_down)
    top_count = expert_ids.shape[1]
    model_width = normed.shape[1]
    sp_count = lax.axis_size("sp")
    tp_count = lax.axis_size("tp")
    expert_total = sp_count * tp_count
    pair_count = tok_dev * top_count
    capacity = max(2, 2 * pair_count // expert_total)
    flat_ids = expert_ids.reshape(-1)
    one_hot = (flat_ids[:, None] == jnp.arange(expert_total, dtype=jnp.int32)[None, :]).astype(
        jnp.int32
    )
    pair_rank = jnp.sum((jnp.cumsum(one_hot, axis=0) - one_hot) * one_hot, axis=1)
    pair_token = jnp.arange(pair_count, dtype=jnp.int32) // top_count
    send_rows = (
        jnp.zeros((expert_total, capacity, model_width), jnp.bfloat16)
        .at[flat_ids, pair_rank]
        .set(normed[pair_token])
    )
    arrived = lax.all_to_all(send_rows, ("sp", "tp"), split_axis=0, concat_axis=0, tiled=True)
    arrived_shape = arrived.shape
    flat_rows = arrived.reshape(-1, arrived_shape[-1])
    result = swiglu_rows(flat_rows, gate_experts[0], up_experts[0], down_experts[0]).astype(
        jnp.bfloat16
    )
    finished = result.reshape(arrived_shape)
    returned = lax.all_to_all(finished, ("sp", "tp"), split_axis=0, concat_axis=0, tiled=True)
    chosen = returned[flat_ids, pair_rank].reshape(tok_dev, top_count, model_width)
    routed = jnp.sum(chosen.astype(jnp.float32) * expert_mix[:, :, None], axis=1)
    return (middle_f + shared + routed).astype(jnp.bfloat16)


def solution(mesh):
    in_specs = (
        P(("sp", "tp"), None),
        P("sp", "tp", None),
        P("sp", "tp", None),
        P("sp", "tp", None),
        P("sp", "tp", None),
        P("sp", "tp", None),
        P("sp", "tp", None),
        P("tp"),
        P("tp"),
        P(),
        P(),
        P(),
        P(("sp", "tp"), None),
        P(("sp", "tp"), None),
        P(("sp", "tp"), None, None),
        P(("sp", "tp"), None, None),
        P(("sp", "tp"), None, None),
        P(),
        P(),
        P(),
    )
    out_specs = P(("sp", "tp"), None)
    return jax.shard_map(
        per_device, mesh=mesh, in_specs=in_specs, out_specs=out_specs, check_vma=False
    )
```

profile of v0, /device:TPU:0, one launch (start us, length us, event | category | flops | bytes accessed | tf_op | source)
XLA Modules:
  0.0 333.9 jit_solution(18437636033774966400)
XLA Ops:
  6.5 0.7 all-gather.2.cloned.1.call-update
  7.3 33.6 %all_gather.12 = bf16[2048,1,128]{2,0,1:T(8,128)(2,1)S(1)} all-gather(bf16[256,1,128]{2,0,1:T(8,128)(2,1)} %param.22), channel_id=1, replica_groups=mesh['sp'=8,'tp'=4] {'sp'}, dimensions={0}, use_global_device_ids=true | all-gather | bytes 589824 | tf_op jit(solution)/shard_map/all_gather | solution.py:107
  40.9 0.8 copy.35
  41.6 0.1 eq.29
  41.8 0.6 reduce-window.6
  42.4 0.2 slice_reduce_fusion
  42.6 0.1 eq.25
  42.7 0.1 reshape.406
  44.1 0.1 fusion.73
  44.2 2.8 fusion.88
  47.0 1.8 fusion.89
  48.9 31.4 %all_gather.15 = bf16[2048,1,128]{2,0,1:T(8,128)(2,1)S(1)} all-gather(bf16[256,1,128]{2,0,1:T(8,128)(2,1)S(1)} %copy-done.5), channel_id=1, replica_groups=mesh['sp'=8,'tp'=4] {'sp'}, dimensions={0}, use_global_device_ids=true | all-gather | bytes 589824 | tf_op jit(solution)/shard_map/all_gather | solution.py:110
  80.3 31.5 %all_gather.13 = bf16[2048,1,128]{2,0,1:T(8,128)(2,1)S(1)} all-gather(bf16[256,1,128]{2,0,1:T(8,128)(2,1)S(1)} %copy-done.6), channel_id=1, replica_groups=mesh['sp'=8,'tp'=4] {'sp'}, dimensions={0}, use_global_device_ids=true | all-gather | bytes 589824 | tf_op jit(solution)/shard_map/all_gather | solution.py:108
  111.8 1.8 fusion.91
  113.6 1.8 fusion.90
  115.4 2.1 fusion.19
  117.5 0.7 fusion.38
  118.2 0.7 multiply_reduce_fusion.2
  118.9 0.7 fusion.32
  119.6 0.7 multiply_reduce_fusion.3
  120.4 0.6 broadcast.531
  121.0 0.7 reduce.22
  121.7 0.1 copy.50
  121.8 0.7 reshape.432
  122.5 3.3 all-to-all-start.1
  125.8 0.7 reduce.23
  126.5 0.1 copy.51
  126.6 0.6 reshape.434
  127.3 2.6 all-to-all-done.1
  129.9 3.3 all-to-all-start
  133.3 3.9 %all-to-all-done = bf16[4,2,4096]{2,1,0:T(2,128)(2,1)S(1)} async-done(((bf16[4,2,4096]{2,1,0:T(2,128)(2,1)}), bf16[4,2,4096]{2,1,0:T(2,128)(2,1)S(1)}, u32[]{:S(2)}, u32[]{:S(2)}) %all-to-all-start) | async-done | bytes 65568 | tf_op jit(solution)/shard_map/all_to_all | solution.py:139
  137.4 3.2 multiply_reduce_fusion.1
  140.6 0.1 multiply_convert_fusion.1
  140.7 2.3 gather_fusion
  143.1 1.6 broadcast_in_dim.49
  144.7 46.2 %scatter_fusion = bf16[32,16,2048]{2,1,0:T(8,128)(2,1)} fusion(bf16[32,16,2048]{2,1,0:T(8,128)(2,1)} %broadcast_in_dim.49, s32[256]{0:T(256)S(1)} %bitcast.169, bf16[256,2048]{1,0:T(8,128)(2,1)} %gather_fusion), kind=kCustom, calls=%fused_computation.2 | custom fusion | bytes 3147776 | tf_op jit(solution)/shard_map/scatter | solution.py:168
  190.9 53.7 %all_to_all.40 = bf16[32,16,2048]{2,1,0:T(8,128)(2,1)S(1)} all-to-all(bf16[32,16,2048]{2,1,0:T(8,128)(2,1)} %scatter_fusion), channel_id=1, replica_groups=mesh['sp'=8,'tp'=4] {'sp','tp'}, dimensions={0} | all-to-all | bytes 4194304 | tf_op jit(solution)/shard_map/all_to_all | solution.py:170
  244.6 1.3 copy-done.3
  246.0 3.6 %fusion.4 = f32[512,1024]{1,0:T(8,128)} fusion(bf16[512,2048]{1,0:T(8,128)(2,1)S(1)} %bitcast.171, bf16[1,2048,1024]{2,1,0:T(8,128)(2,1)S(1)} %copy-done.10), kind=kOutput, calls=%fused_computation.7 | convolution fusion | flops 2147483648 | bytes 8388608 | tf_op jit(solution)/shard_map/dot_general | solution.py:14
  249.6 10.6 %fusion.6 = bf16[512,2048]{1,0:T(8,128)(2,1)} fusion(bf16[1,1024,2048]{2,1,0:T(8,128)(2,1)} %param.36, f32[512,1024]{1,0:T(8,128)} %fusion.4, bf16[512,2048]{1,0:T(8,128)(2,1)} %bitcast.172, bf16[1,2048,1024]{2,1,0:T(8,128)(2,1)} %param.35), kind=kOutput, calls=%fused_computation.9 | convolution fusion | flops 4299161600 | bytes 14680064 | tf_op jit(solution)/shard_map/dot_general | solution.py:17
  260.2 3.8 %all-to-all-start.3 = ((bf16[32,16,2048]{2,1,0:T(8,128)(2,1)}), bf16[32,16,2048]{2,1,0:T(8,128)(2,1)}, u32[]{:S(2)}, u32[]{:S(2)}) async-start(bf16[32,16,2048]{2,1,0:T(8,128)(2,1)} %bitcast.170), calls=%async_computation.3 | async-start | bytes 4194304 | tf_op jit(solution)/shard_map/all_to_all | solution.py:177
  264.0 0.7 copy.39
  264.7 2.1 fusion.92
  266.8 45.9 %all-to-all-done.3 = bf16[32,16,2048]{2,1,0:T(8,128)(2,1)} async-done(((bf16[32,16,2048]{2,1,0:T(8,128)(2,1)}), bf16[32,16,2048]{2,1,0:T(8,128)(2,1)}, u32[]{:S(2)}, u32[]{:S(2)}) %all-to-all-start.3) | async-done | bytes 2097184 | tf_op jit(solution)/shard_map/all_to_all | solution.py:177
  312.7 5.1 %gather_fusion.1 = bf16[256,2048]{1,0:T(8,128)(2,1)} fusion(bf16[32,16,2048]{2,1,0:T(8,128)(2,1)} %all-to-all-done.3, s32[256]{0:T(256)S(1)} %bitcast.168), kind=kCustom, calls=%fused_computation.1 | custom fusion | bytes 2099200 | tf_op jit(solution)/shard_map/gather | solution.py:178
  317.9 2.7 reshape.410
  320.6 3.2 multiply_reduce_fusion
  323.8 3.2 fusion.14
  (52 shorter events, 0.6 us)
Async XLA Ops:
  6.5 317.3 %copy-start = (bf16[512,2048]{1,0:T(8,128)(2,1)S(1)}, bf16[512,2048]{1,0:T(8,128)(2,1)}, u32[]{:S(2)}) copy-start(bf16[512,2048]{1,0:T(8,128)(2,1)} %param.39) | copy-start | bytes 6291460
  6.5 40.5 %copy-start.12 = (bf16[256,1,128]{2,0,1:T(8,128)(2,1)S(1)}, bf16[256,1,128]{2,0,1:T(8,128)(2,1)}, u32[]{:S(2)}) copy-start(bf16[256,1,128]{2,0,1:T(8,128)(2,1)} %param.21) | copy-start | bytes 196612
  6.5 105.2 %all-gather.2.cloned.1.call-start = ((), (), s32[]{:S(2)}) async-start(), calls=%async_computation.4 | async-start | bytes 1179648 | tf_op jit(solution)/shard_map/all_gather | solution.py:109
  47.0 1.9 copy-start.5
  47.0 33.3 %copy-start.6 = (bf16[256,1,128]{2,0,1:T(8,128)(2,1)S(1)}, bf16[256,1,128]{2,0,1:T(8,128)(2,1)}, u32[]{:S(2)}) copy-start(bf16[256,1,128]{2,0,1:T(8,128)(2,1)} %param.23) | copy-start | bytes 196612
  47.0 64.8 %copy-start.11 = (bf16[256,1,256]{2,0,1:T(8,128)(2,1)S(1)}, bf16[256,1,256]{2,0,1:T(8,128)(2,1)}, u32[]{:S(2)}) copy-start(bf16[256,1,256]{2,0,1:T(8,128)(2,1)} %param.24) | copy-start | bytes 393220
  111.8 3.6 %copy-start.2 = (f32[256,2048]{1,0:T(8,128)S(1)}, f32[256,2048]{1,0:T(8,128)}, u32[]{:S(2)}) copy-start(f32[256,2048]{1,0:T(8,128)} %get-tuple-element.62) | copy-start | bytes 6291460
  113.6 1.8 copy-start.1
  119.6 0.7 copy-start.9
  120.3 17.1 %copy-start.4 = (bf16[64,2048]{1,0:T(8,128)(2,1)S(1)}, bf16[64,2048]{1,0:T(8,128)(2,1)}, u32[]{:S(2)}) copy-start(bf16[64,2048]{1,0:T(8,128)(2,1)} %param.20) | copy-start | bytes 786436
  122.5 7.4 %all-to-all-start.1 = ((bf16[4,2,4096]{2,1,0:T(2,128)(2,1)}), bf16[4,2,4096]{2,1,0:T(2,128)(2,1)S(1)}, u32[]{:S(2)}, u32[]{:S(2)}) async-start(bf16[4,2,4096]{2,1,0:T(2,128)(2,1)} %reshape.432), calls=%async_computation.1 | async-start | bytes 131072 | tf_op jit(solution)/shard_map/all_to_all | solution.py:140
  129.9 7.4 %all-to-all-start = ((bf16[4,2,4096]{2,1,0:T(2,128)(2,1)}), bf16[4,2,4096]{2,1,0:T(2,128)(2,1)S(1)}, u32[]{:S(2)}, u32[]{:S(2)}) async-start(bf16[4,2,4096]{2,1,0:T(2,128)(2,1)} %reshape.434), calls=%async_computation | async-start | bytes 131072 | tf_op jit(solution)/shard_map/all_to_all | solution.py:139
  137.4 3.2 copy-start.7
  190.9 55.0 %copy-start.10 = (bf16[1,2048,1024]{2,1,0:T(8,128)(2,1)S(1)}, bf16[1,2048,1024]{2,1,0:T(8,128)(2,1)}, u32[]{:S(2)}) copy-start(bf16[1,2048,1024]{2,1,0:T(8,128)(2,1)} %param.34) | copy-start | bytes 12582916
  244.6 1.3 copy-start.3
  260.2 3.8 %copy-start.8 = (f32[64,4]{0,1:T(4,128)S(1)}, f32[64,4]{0,1:T(4,128)}, u32[]{:S(2)}) copy-start(f32[64,4]{0,1:T(4,128)} %param.33) | copy-start | bytes 3076
  260.2 52.5 %all-to-all-start.3 = ((bf16[32,16,2048]{2,1,0:T(8,128)(2,1)}), bf16[32,16,2048]{2,1,0:T(8,128)(2,1)}, u32[]{:S(2)}, u32[]{:S(2)}) async-start(bf16[32,16,2048]{2,1,0:T(8,128)(2,1)} %bitcast.170), calls=%async_computation.3 | async-start | bytes 4194304 | tf_op jit(solution)/shard_map/all_to_all | solution.py:177
Sparse Core Ops, SparseCore 0:
  9.5 43.6 all-gather.1
where the time goes:
time: 336 us; the launch traced here: 334 us
  blocking collectives  150 us (45%)
  local copies, waits for them, and re-layouts  63.9 us (19%)
  waiting for transfers between devices  53.1 us (16%)
  matrix products  33.6 us (10%)
  between operations  15.1 us (4%)
  starting transfers between devices  10.4 us (3%)
  other arithmetic  7.7 us (2%)
    all_to_all x1, blocking collectives, per_device(): lax.all_to_all(send_rows, ('sp', 'tp'), split_axis=0, concat_axis=0, tile...  53.7 us
    scatter x1, local copies, waits for them, and re-layouts, per_device(): send_rows = jnp.zeros((expert_total, capacity, model_width), jnp.bfloat16...  46.2 us
    all_to_all x1, waiting for transfers between devices, per_device(): lax.all_to_all(finished, ('sp', 'tp'), split_axis=0, concat_axis=0, tiled...  45.9 us
    all_gather x1, blocking collectives, per_device(): key_piece_a = lax.all_gather(key_a, 'sp', axis=0, tiled=True)  33.6 us
    all_gather x1, blocking collectives, per_device(): value_piece_a = lax.all_gather(value_a, 'sp', axis=0, tiled=True)  31.5 us
    all_gather x1, blocking collectives, per_device(): value_piece_b = lax.all_gather(value_b, 'sp', axis=0, tiled=True)  31.4 us
    dot_general x2, matrix products, swiglu_rows(): return jnp.dot(hidden, w_down, preferred_element_type=jnp.float32)  13.8 us
    dot_general x4, matrix products, online_update(): jnp.einsum('qhd,khd->hqk', query_map, key_map, preferred_element_type=jnp...  8.17 us
  transfers between devices with their start and end apart: 4, of which 3 were waited for; matrix products, arithmetic and copies ran while one was open for 3% of the time, Pallas kernels for 0%

commit v1 on v0

--- a/solution.py
+++ b/solution.py
@@ -104,7 +104,22 @@
         empty_state(query_rows, query_a.shape[1], value_width),
         empty_state(query_rows, query_b.shape[1], value_width),
     )
-    key_piece_a = lax.all_gather(key_a, "sp", axis=0, tiled=True)
+    ways, here, step = (lax.axis_size("sp"), lax.axis_index("sp"), key_a.shape[0])
+    shape = [n * ways if d == 0 else n for d, n in enumerate(key_a.shape)]
+    key_piece_a = lax.dynamic_update_slice_in_dim(
+        jnp.zeros(shape, key_a.dtype), key_a, here * step, axis=0
+    )
+    going_up = going_down = key_a
+    for far in range(1, ways // 2 + 1):
+        going_up = lax.ppermute(going_up, "sp", [(d, (d + 1) % ways) for d in range(ways)])
+        key_piece_a = lax.dynamic_update_slice_in_dim(
+            key_piece_a, going_up, (here - far) % ways * step, axis=0
+        )
+        if 2 * far < ways:
+            going_down = lax.ppermute(going_down, "sp", [(d, (d - 1) % ways) for d in range(ways)])
+            key_piece_a = lax.dynamic_update_slice_in_dim(
+                key_piece_a, going_down, (here + far) % ways * step, axis=0
+            )
     value_piece_a = lax.all_gather(value_a, "sp", axis=0, tiled=True)
     key_piece_b = lax.all_gather(key_b, "sp", axis=0, tiled=True)
     value_piece_b = lax.all_gather(value_b, "sp", axis=0, tiled=True)

time: 336 us -> 331 us (0.985)
  blocking collectives: 150 us -> 117 us
  starting transfers between devices: 10.4 us -> 25.9 us
  waiting for transfers between devices: 53.1 us -> 60.2 us
  local copies, waits for them, and re-layouts: 63.9 us -> 69.7 us
    all_gather x1 -> x0, blocking collectives: 33.6 us -> none  [per_device(): key_piece_a = lax.all_gather(key_a, 'sp', axis=0, tiled=True)]
    ppermute x0 -> x7, starting transfers between devices: none -> 15.6 us  [the longest x3 12.5 us: per_device(): lax.ppermute(going_down, 'sp', [(d, (d - 1) % ways) for d in range(ways)])]
    ppermute x0 -> x7, waiting for transfers between devices: none -> 7.71 us  [the longest x4 7.71 us: per_device(): lax.ppermute(going_up, 'sp', [(d, (d + 1) % ways) for d in range(ways)])]
    dynamic_update_slice x0 -> x8, local copies, waits for them, and re-layouts: none -> 4.98 us  [the longest x4 2.5 us: per_device(): lax.dynamic_update_slice_in_dim(key_piece_a, going_up, (here - far) % way...]
  transfers between devices with their start and end apart: 4 -> 11, of which waited for: 3 -> 6; matrix products, arithmetic and copies ran while one was open for 3% -> 6% of each run, Pallas kernels for 0% -> 0%
where the time goes in v1:
time: 331 us; the launch traced here: 329 us
  blocking collectives  117 us (35%)
  local copies, waits for them, and re-layouts  69.7 us (21%)
  waiting for transfers between devices  60.2 us (18%)
  matrix products  34.4 us (10%)
  starting transfers between devices  25.9 us (8%)
  between operations  15.3 us (5%)
  other arithmetic  7.11 us (2%)
    all_to_all x1, blocking collectives, per_device(): lax.all_to_all(send_rows, ('sp', 'tp'), split_axis=0, concat_axis=0, tile...  51.9 us
    scatter x1, local copies, waits for them, and re-layouts, per_device(): send_rows = jnp.zeros((expert_total, capacity, model_width), jnp.bfloat16...  46.2 us
    all_to_all x1, waiting for transfers between devices, per_device(): lax.all_to_all(finished, ('sp', 'tp'), split_axis=0, concat_axis=0, tiled...  45.9 us
    all_gather x1, blocking collectives, per_device(): value_piece_b = lax.all_gather(value_b, 'sp', axis=0, tiled=True)  32.8 us
    all_gather x1, blocking collectives, per_device(): value_piece_a = lax.all_gather(value_a, 'sp', axis=0, tiled=True)  32 us
    dot_general x2, matrix products, swiglu_rows(): return jnp.dot(hidden, w_down, preferred_element_type=jnp.float32)  13.8 us
    ppermute x3, starting transfers between devices, per_device(): lax.ppermute(going_down, 'sp', [(d, (d - 1) % ways) for d in range(ways)])  12.5 us
    dot_general x4, matrix products, online_update(): jnp.einsum('qhd,khd->hqk', query_map, key_map, preferred_element_type=jnp...  9.31 us
  transfers between devices with their start and end apart: 11, of which 6 were waited for; matrix products, arithmetic and copies ran while one was open for 6% of the time, Pallas kernels for 0%

profile of v1, /device:TPU:0, one launch (start us, length us, event | category | flops | bytes accessed | tf_op | source)
XLA Modules:
  0.0 329.3 jit_solution(9653954770351036120)
XLA Ops:
  6.5 3.0 collective-permute-start
  9.6 3.1 collective-permute-start.1
  12.7 0.8 copy.41
  13.7 32.8 %all_gather.11 = bf16[2048,1,128]{2,0,1:T(8,128)(2,1)S(1)} all-gather(bf16[256,1,128]{2,0,1:T(8,128)(2,1)} %param.26), channel_id=1, replica_groups=mesh['sp'=8,'tp'=4] {'sp'}, dimensions={0}, use_global_device_ids=true | all-gather | bytes 589824 | tf_op jit(solution)/shard_map/all_gather | solution.py:125
  46.5 32.0 %all_gather.9 = bf16[2048,1,128]{2,0,1:T(8,128)(2,1)S(1)} all-gather(bf16[256,1,128]{2,0,1:T(8,128)(2,1)} %param.23), channel_id=1, replica_groups=mesh['sp'=8,'tp'=4] {'sp'}, dimensions={0}, use_global_device_ids=true | all-gather | bytes 589824 | tf_op jit(solution)/shard_map/all_gather | solution.py:123
  79.4 0.9 broadcast_in_dim.50
  80.3 0.6 constant_dynamic-update-slice_fusion.7
  82.7 4.7 %collective-permute-start.3 = (bf16[256,1,128]{2,0,1:T(8,128)(2,1)S(1)}, bf16[256,1,128]{2,0,1:T(8,128)(2,1)S(1)}, u32[]{:S(2)}, u32[]{:S(2)}) collective-permute-start(bf16[256,1,128]{2,0,1:T(8,128)(2,1)S(1)} %collective-permute-done.1), channel_id=1, source_target_pairs={{0,28},{4,0},{8,4},{12,8},{16,12},{20,16},{24,20},{28,24},{1,29},{... | collective-permute-start | bytes 196616 | tf_op jit(solution)/shard_map/ppermute | solution.py:119
  87.4 0.6 constant_dynamic-update-slice_fusion.6
  88.0 0.6 constant_dynamic-update-slice_fusion.5
  88.6 1.0 collective-permute-done.2
  89.6 4.7 %collective-permute-start.5 = (bf16[256,1,128]{2,0,1:T(8,128)(2,1)S(1)}, bf16[256,1,128]{2,0,1:T(8,128)(2,1)S(1)}, u32[]{:S(2)}, u32[]{:S(2)}) collective-permute-start(bf16[256,1,128]{2,0,1:T(8,128)(2,1)S(1)} %collective-permute-done.3), channel_id=1, source_target_pairs={{0,28},{4,0},{8,4},{12,8},{16,12},{20,16},{24,20},{28,24},{1,29},{... | collective-permute-start | bytes 196616 | tf_op jit(solution)/shard_map/ppermute | solution.py:119
  94.3 0.6 constant_dynamic-update-slice_fusion.4
  95.0 0.6 constant_dynamic-update-slice_fusion.3
  95.6 1.0 collective-permute-done.4
  96.6 0.6 constant_dynamic-update-slice_fusion.2
  97.2 0.6 constant_dynamic-update-slice_fusion.1
  97.8 5.7 %collective-permute-done.6 = bf16[256,1,128]{2,0,1:T(8,128)(2,1)S(1)} collective-permute-done((bf16[256,1,128]{2,0,1:T(8,128)(2,1)S(1)}, bf16[256,1,128]{2,0,1:T(8,128)(2,1)S(1)}, u32[]{:S(2)}, u32[]{:S(2)}) %collective-permute-start.6) | collective-permute-done | bytes 65568 | tf_op jit(solution)/shard_map/ppermute | solution.py:114
  103.5 0.6 constant_dynamic-update-slice_fusion
  104.2 2.9 fusion.97
  107.1 3.0 fusion.96
  110.1 1.7 fusion.99
  111.8 1.7 fusion.98
  113.6 1.5 fusion.21
  118.3 0.7 reduce.22
  119.1 0.7 reshape.432
  119.7 3.3 all-to-all-start.1
  123.1 0.7 reduce.23
  123.9 0.6 reshape.434
  124.5 2.6 all-to-all-done.1
  127.1 3.3 all-to-all-start
  130.6 3.9 %all-to-all-done = bf16[4,2,4096]{2,1,0:T(2,128)(2,1)S(1)} async-done(((bf16[4,2,4096]{2,1,0:T(2,128)(2,1)}), bf16[4,2,4096]{2,1,0:T(2,128)(2,1)S(1)}, u32[]{:S(2)}, u32[]{:S(2)}) %all-to-all-start) | async-done | bytes 65568 | tf_op jit(solution)/shard_map/all_to_all | solution.py:154
  134.7 3.2 multiply_reduce_fusion.1
  138.0 2.3 gather_fusion
  140.3 1.6 broadcast_in_dim.53
  142.0 46.2 %scatter_fusion = bf16[32,16,2048]{2,1,0:T(8,128)(2,1)} fusion(bf16[32,16,2048]{2,1,0:T(8,128)(2,1)} %broadcast_in_dim.53, s32[256]{0:T(256)S(1)} %bitcast.177, bf16[256,2048]{1,0:T(8,128)(2,1)} %gather_fusion), kind=kCustom, calls=%fused_computation.2 | custom fusion | bytes 3147776 | tf_op jit(solution)/shard_map/scatter | solution.py:183
  188.2 51.9 %all_to_all.40 = bf16[32,16,2048]{2,1,0:T(8,128)(2,1)S(1)} all-to-all(bf16[32,16,2048]{2,1,0:T(8,128)(2,1)} %scatter_fusion), channel_id=1, replica_groups=mesh['sp'=8,'tp'=4] {'sp','tp'}, dimensions={0} | all-to-all | bytes 4194304 | tf_op jit(solution)/shard_map/all_to_all | solution.py:185
  240.1 1.3 copy-done.3
  241.4 3.6 %fusion.4 = f32[512,1024]{1,0:T(8,128)} fusion(bf16[512,2048]{1,0:T(8,128)(2,1)S(1)} %bitcast.179, bf16[1,2048,1024]{2,1,0:T(8,128)(2,1)S(1)} %copy-done.9), kind=kOutput, calls=%fused_computation.7 | convolution fusion | flops 2147483648 | bytes 8388608 | tf_op jit(solution)/shard_map/dot_general | solution.py:14
  245.1 10.6 %fusion.6 = bf16[512,2048]{1,0:T(8,128)(2,1)} fusion(bf16[1,1024,2048]{2,1,0:T(8,128)(2,1)} %param.36, f32[512,1024]{1,0:T(8,128)} %fusion.4, bf16[512,2048]{1,0:T(8,128)(2,1)} %bitcast.180, bf16[1,2048,1024]{2,1,0:T(8,128)(2,1)} %param.35), kind=kOutput, calls=%fused_computation.9 | convolution fusion | flops 4299161600 | bytes 14680064 | tf_op jit(solution)/shard_map/dot_general | solution.py:17
  255.7 3.7 %all-to-all-start.3 = ((bf16[32,16,2048]{2,1,0:T(8,128)(2,1)}), bf16[32,16,2048]{2,1,0:T(8,128)(2,1)}, u32[]{:S(2)}, u32[]{:S(2)}) async-start(bf16[32,16,2048]{2,1,0:T(8,128)(2,1)} %bitcast.178), calls=%async_computation.3 | async-start | bytes 4194304 | tf_op jit(solution)/shard_map/all_to_all | solution.py:192
  259.4 0.7 copy.45
  260.1 2.1 fusion.100
  262.2 45.9 %all-to-all-done.3 = bf16[32,16,2048]{2,1,0:T(8,128)(2,1)} async-done(((bf16[32,16,2048]{2,1,0:T(8,128)(2,1)}), bf16[32,16,2048]{2,1,0:T(8,128)(2,1)}, u32[]{:S(2)}, u32[]{:S(2)}) %all-to-all-start.3) | async-done | bytes 2097184 | tf_op jit(solution)/shard_map/all_to_all | solution.py:192
  308.1 5.1 %gather_fusion.1 = bf16[256,2048]{1,0:T(8,128)(2,1)} fusion(bf16[32,16,2048]{2,1,0:T(8,128)(2,1)} %all-to-all-done.3, s32[256]{0:T(256)S(1)} %bitcast.176), kind=kCustom, calls=%fused_computation.1 | custom fusion | bytes 2099200 | tf_op jit(solution)/shard_map/gather | solution.py:193
  313.3 2.7 reshape.410
  316.0 3.2 multiply_reduce_fusion
  319.2 3.2 fusion.16
  (71 shorter events, 5.1 us)
Async XLA Ops:
  6.5 312.7 %copy-start = (bf16[512,2048]{1,0:T(8,128)(2,1)S(1)}, bf16[512,2048]{1,0:T(8,128)(2,1)}, u32[]{:S(2)}) copy-start(bf16[512,2048]{1,0:T(8,128)(2,1)} %param.39) | copy-start | bytes 6291460
  6.5 73.8 %copy-start.5 = (bf16[256,1,128]{2,0,1:T(8,128)(2,1)S(1)}, bf16[256,1,128]{2,0,1:T(8,128)(2,1)}, u32[]{:S(2)}) copy-start(bf16[256,1,128]{2,0,1:T(8,128)(2,1)} %param.22) | copy-start | bytes 196612
  6.5 97.6 %copy-start.11 = (bf16[256,1,128]{2,0,1:T(8,128)(2,1)S(1)}, bf16[256,1,128]{2,0,1:T(8,128)(2,1)}, u32[]{:S(2)}) copy-start(bf16[256,1,128]{2,0,1:T(8,128)(2,1)} %param.21) | copy-start | bytes 196612
  6.5 103.5 %all-gather.2.cloned.1.call-start = ((), (), s32[]{:S(2)}) async-start(), calls=%async_computation.4 | async-start | bytes 1179648 | tf_op jit(solution)/shard_map/all_gather | solution.py:124
  6.5 76.1 %collective-permute-start = (bf16[256,1,128]{2,0,1:T(8,128)(2,1)}, bf16[256,1,128]{2,0,1:T(8,128)(2,1)S(1)}, u32[]{:S(2)}, u32[]{:S(2)}) collective-permute-start(bf16[256,1,128]{2,0,1:T(8,128)(2,1)} %param.22), channel_id=1, source_target_pairs={{0,4},{4,8},{8,12},{12,16},{16,20},{20,24},{24,28},{28,0},{1,5},{5... | collective-permute-start | bytes 196616 | tf_op jit(solution)/shard_map/ppermute | solution.py:114
  9.6 73.1 %collective-permute-start.1 = (bf16[256,1,128]{2,0,1:T(8,128)(2,1)}, bf16[256,1,128]{2,0,1:T(8,128)(2,1)S(1)}, u32[]{:S(2)}, u32[]{:S(2)}) collective-permute-start(bf16[256,1,128]{2,0,1:T(8,128)(2,1)} %param.22), channel_id=1, source_target_pairs={{0,28},{4,0},{8,4},{12,8},{16,12},{20,16},{24,20},{28,24},{1,29},{... | collective-permute-start | bytes 196616 | tf_op jit(solution)/shard_map/ppermute | solution.py:119
  82.6 7.0 %collective-permute-start.2 = (bf16[256,1,128]{2,0,1:T(8,128)(2,1)S(1)}, bf16[256,1,128]{2,0,1:T(8,128)(2,1)S(1)}, u32[]{:S(2)}, u32[]{:S(2)}) collective-permute-start(bf16[256,1,128]{2,0,1:T(8,128)(2,1)S(1)} %collective-permute-done), channel_id=1, source_target_pairs={{0,4},{4,8},{8,12},{12,16},{16,20},{20,24},{24,28},{28,0},{1,5},{5... | collective-permute-start | bytes 196616 | tf_op jit(solution)/shard_map/ppermute | solution.py:114
  82.7 6.9 %collective-permute-start.3 = (bf16[256,1,128]{2,0,1:T(8,128)(2,1)S(1)}, bf16[256,1,128]{2,0,1:T(8,128)(2,1)S(1)}, u32[]{:S(2)}, u32[]{:S(2)}) collective-permute-start(bf16[256,1,128]{2,0,1:T(8,128)(2,1)S(1)} %collective-permute-done.1), channel_id=1, source_target_pairs={{0,28},{4,0},{8,4},{12,8},{16,12},{20,16},{24,20},{28,24},{1,29},{... | collective-permute-start | bytes 196616 | tf_op jit(solution)/shard_map/ppermute | solution.py:119
  89.6 7.0 %collective-permute-start.4 = (bf16[256,1,128]{2,0,1:T(8,128)(2,1)S(1)}, bf16[256,1,128]{2,0,1:T(8,128)(2,1)S(1)}, u32[]{:S(2)}, u32[]{:S(2)}) collective-permute-start(bf16[256,1,128]{2,0,1:T(8,128)(2,1)S(1)} %collective-permute-done.2), channel_id=1, source_target_pairs={{0,4},{4,8},{8,12},{12,16},{16,20},{20,24},{24,28},{28,0},{1,5},{5... | collective-permute-start | bytes 196616 | tf_op jit(solution)/shard_map/ppermute | solution.py:114
  89.6 7.6 %collective-permute-start.5 = (bf16[256,1,128]{2,0,1:T(8,128)(2,1)S(1)}, bf16[256,1,128]{2,0,1:T(8,128)(2,1)S(1)}, u32[]{:S(2)}, u32[]{:S(2)}) collective-permute-start(bf16[256,1,128]{2,0,1:T(8,128)(2,1)S(1)} %collective-permute-done.3), channel_id=1, source_target_pairs={{0,28},{4,0},{8,4},{12,8},{16,12},{20,16},{24,20},{28,24},{1,29},{... | collective-permute-start | bytes 196616 | tf_op jit(solution)/shard_map/ppermute | solution.py:119
  96.6 7.0 %collective-permute-start.6 = (bf16[256,1,128]{2,0,1:T(8,128)(2,1)S(1)}, bf16[256,1,128]{2,0,1:T(8,128)(2,1)S(1)}, u32[]{:S(2)}, u32[]{:S(2)}) collective-permute-start(bf16[256,1,128]{2,0,1:T(8,128)(2,1)S(1)} %collective-permute-done.4), channel_id=1, source_target_pairs={{0,4},{4,8},{8,12},{12,16},{16,20},{20,24},{24,28},{28,0},{1,5},{5... | collective-permute-start | bytes 196616 | tf_op jit(solution)/shard_map/ppermute | solution.py:114
  107.1 3.0 copy-start.10
  110.1 3.5 %copy-start.2 = (f32[256,2048]{0,1:T(8,128)S(1)}, f32[256,2048]{0,1:T(8,128)}, u32[]{:S(2)}) copy-start(f32[256,2048]{0,1:T(8,128)} %get-tuple-element.62) | copy-start | bytes 6291460
  111.8 1.8 copy-start.1
  116.9 0.7 copy-start.8
  117.5 17.1 %copy-start.4 = (bf16[64,2048]{1,0:T(8,128)(2,1)S(1)}, bf16[64,2048]{1,0:T(8,128)(2,1)}, u32[]{:S(2)}) copy-start(bf16[64,2048]{1,0:T(8,128)(2,1)} %param.20) | copy-start | bytes 786436
  119.7 7.4 %all-to-all-start.1 = ((bf16[4,2,4096]{2,1,0:T(2,128)(2,1)}), bf16[4,2,4096]{2,1,0:T(2,128)(2,1)S(1)}, u32[]{:S(2)}, u32[]{:S(2)}) async-start(bf16[4,2,4096]{2,1,0:T(2,128)(2,1)} %reshape.432), calls=%async_computation.1 | async-start | bytes 131072 | tf_op jit(solution)/shard_map/all_to_all | solution.py:155
  127.1 7.4 %all-to-all-start = ((bf16[4,2,4096]{2,1,0:T(2,128)(2,1)}), bf16[4,2,4096]{2,1,0:T(2,128)(2,1)S(1)}, u32[]{:S(2)}, u32[]{:S(2)}) async-start(bf16[4,2,4096]{2,1,0:T(2,128)(2,1)} %reshape.434), calls=%async_computation | async-start | bytes 131072 | tf_op jit(solution)/shard_map/all_to_all | solution.py:154
  134.7 3.2 copy-start.6
  188.2 53.2 %copy-start.9 = (bf16[1,2048,1024]{2,1,0:T(8,128)(2,1)S(1)}, bf16[1,2048,1024]{2,1,0:T(8,128)(2,1)}, u32[]{:S(2)}) copy-start(bf16[1,2048,1024]{2,1,0:T(8,128)(2,1)} %param.34) | copy-start | bytes 12582916
  240.1 1.3 copy-start.3
  255.7 3.7 %copy-start.7 = (f32[64,4]{0,1:T(4,128)S(1)}, f32[64,4]{0,1:T(4,128)}, u32[]{:S(2)}) copy-start(f32[64,4]{0,1:T(4,128)} %param.33) | copy-start | bytes 3076
  255.7 52.4 %all-to-all-start.3 = ((bf16[32,16,2048]{2,1,0:T(8,128)(2,1)}), bf16[32,16,2048]{2,1,0:T(8,128)(2,1)}, u32[]{:S(2)}, u32[]{:S(2)}) async-start(bf16[32,16,2048]{2,1,0:T(8,128)(2,1)} %bitcast.178), calls=%async_computation.3 | async-start | bytes 4194304 | tf_op jit(solution)/shard_map/all_to_all | solution.py:192
Sparse Core Ops, SparseCore 0:
  12.8 42.1 all-gather.1
